TPU v7x, 32 devices: a whole 2x2x4 slice. The times are simulated.
32 devices in a mesh: gr: 2 (over x), fs: 4 (over z), tp: 4 (over y, core).
Axes of the slice: x: 2, y: 2, z: 4, core: 2. Of those that a mesh axis runs over, the one named last changes fastest.
Arguments:
- prompt: bfloat16 [4096, 2048], P(('gr', 'fs', 'tp')), may hold values from -6 to 6
- train_gate: float32 [16, 2048, 256], P(None, ('gr', 'fs'), 'tp'), may hold values from -0.125 to 0.125
- train_up: float32 [16, 2048, 256], P(None, ('gr', 'fs'), 'tp'), may hold values from -0.125 to 0.125
- train_down: float32 [16, 256, 2048], P(None, 'tp', ('gr', 'fs')), may hold values from -0.375 to 0.375
- train_shared_gate: float32 [2048, 256], P(('gr', 'fs'), 'tp'), may hold values from -0.125 to 0.125
- train_shared_up: float32 [2048, 256], P(('gr', 'fs'), 'tp'), may hold values from -0.125 to 0.125
- train_shared_down: float32 [256, 2048], P('tp', ('gr', 'fs')), may hold values from -0.375 to 0.375
- norm_gain: float32 [2048], P(('gr', 'fs')), may hold values from 0.1 to 1.9
- expert_ids: int32 [4096, 8], P(('gr', 'fs', 'tp')), may hold values from 0 to 15, all different within a row; in each aligned block of 128 rows (0 to 127, 128 to 255, ...) at most 65 rows name the same one
- route_weight: float32 [4096, 8], P(('gr', 'fs', 'tp')), may hold values from 0.05 to 0.6
Outputs:
- serve_gate: bfloat16 [16, 2048, 256], P(('fs', 'tp'))
- serve_up: bfloat16 [16, 2048, 256], P(('fs', 'tp'))
- serve_down: bfloat16 [16, 256, 2048], P(('fs', 'tp'))
- serve_shared_gate: bfloat16 [2048, 256], P(None, 'tp')
- serve_shared_up: bfloat16 [2048, 256], P(None, 'tp')
- serve_shared_down: bfloat16 [256, 2048], P('tp')
- mixed_out: bfloat16 [4096, 2048], P(('gr', 'fs', 'tp'))
Inputs may be any that keep to these rules, and one draw needn't show every extreme that they name: `expert_ids`: each row names 8 different experts. Among the rows of one device no expert is named by more than 65 rows, and in some device's rows one expert is named by exactly 65.
All inputs are finite; a program needn't handle non-finite values.
Results may differ from a plain program's by a relative error of at most 0.012.
Values may be sent and summed in bfloat16 or wider, within the bound.
No kernel may reach another device: no remote copies, remote signals or barrier semaphores. Data moves between devices by JAX's collectives and lax.ppermute only.
A program may use at most 128 MiB of HBM per device.

v0:
```python
import jax
import jax.numpy as jnp
from jax import lax
from jax.sharding import PartitionSpec as P

eps_norm = 1e-06
row_tile = 8


def to_owners(pieces):
    count, kinds, hidden_part, width_part = pieces.shape
    fs, tp = (lax.axis_size("fs"), lax.axis_size("tp"))
    pieces = lax.all_to_all(pieces, ("fs", "tp"), split_axis=0, concat_axis=0, tiled=True)
    pieces = pieces.reshape(fs, tp, kinds, hidden_part, width_part)
    pieces = pieces.transpose(2, 1, 3, 0, 4).reshape(kinds, tp * hidden_part, fs * width_part)
    return lax.all_gather(pieces, "gr", axis=2, tiled=True)


def dot_last(left, right):
    return lax.dot_general(
        left, right, (((1,), (1,)), ((), ())), preferred_element_type=jnp.float32
    )


def gated(rows, gate_up):
    both = dot_last(rows, gate_up)
    hidden = both.shape[1] // 2
    return jax.nn.silu(both[:, :hidden]) * both[:, hidden:]


def dense_mix(normed, expert_ids, route_weight, gate_up, lowered, shared_gate_up, shared_down):
    fs, tp = (lax.axis_size("fs"), lax.axis_size("tp"))
    expert_count = fs * tp
    row_count, model_width = normed.shape
    named = expert_ids[None, :, :] == jnp.arange(expert_count, dtype=jnp.int32)[:, None, None]
    weights = jnp.sum(jnp.where(named, route_weight[None], 0.0), axis=2)
    high = lax.reduce_precision(weights, 8, 7)
    coded = jnp.stack((high, weights - high)).astype(jnp.bfloat16).reshape(-1)
    extra = -(-coded.size // (model_width * row_tile)) * row_tile
    coded = jnp.pad(coded, (0, extra * model_width - coded.size)).reshape(extra, model_width)
    block = lax.all_gather(jnp.concatenate((normed, coded), axis=0), ("fs", "tp"), axis=0)
    height = row_count + extra
    mine = lax.axis_index("fs") * tp + lax.axis_index("tp")
    sent = block[:, row_count:].reshape(expert_count, -1)[:, : 2 * expert_count * row_count]
    sent = sent.reshape(expert_count, 2, expert_count, row_count)
    own = lax.dynamic_index_in_dim(sent, mine, axis=2, keepdims=False).astype(jnp.float32)
    own = (own[:, 0] + own[:, 1])[:, :, None]
    act = gated(block.reshape(-1, model_width), gate_up).reshape(expert_count, height, -1)
    act = (act[:, :row_count] * own).astype(jnp.bfloat16)
    near = lax.dynamic_slice_in_dim(block, lax.axis_index("fs") * tp, tp, axis=0)
    shared_act = gated(near.reshape(-1, model_width), shared_gate_up).astype(jnp.bfloat16)
    shared_act = shared_act.reshape(tp, height, -1)[:, :row_count]
    placed = jnp.zeros((expert_count, row_count, shared_act.shape[2]), jnp.bfloat16)
    placed = lax.dynamic_update_slice_in_dim(placed, shared_act, lax.axis_index("fs") * tp, axis=0)
    act = jnp.concatenate((act, placed), axis=2).reshape(expert_count * row_count, -1)
    down = jnp.concatenate((lowered, shared_down), axis=0)
    partial = jnp.dot(act, down, preferred_element_type=jnp.float32).astype(jnp.bfloat16)
    return lax.psum_scatter(partial, ("fs", "tp"), scatter_dimension=0, tiled=True)


def sparse_mix(normed, expert_ids, route_weight, gate_up, lowered, shared_gate_up, shared_down):
    block_rows = lax.all_gather(normed, "tp", axis=0, tiled=True)
    shared_act = gated(block_rows, shared_gate_up).astype(jnp.bfloat16)
    shared_sum = lax.psum_scatter(
        jnp.dot(shared_act, shared_down, preferred_element_type=jnp.float32).astype(jnp.bfloat16),
        "tp",
        scatter_dimension=0,
        tiled=True,
    ).astype(jnp.float32)
    row_count, model_width = normed.shape
    top_count = expert_ids.shape[1]
    expert_count = lax.axis_size("fs") * lax.axis_size("tp")
    capacity = row_count * top_count // expert_count + 1
    flat_ids = expert_ids.reshape(-1)
    onehot = (flat_ids[:, None] == jnp.arange(expert_count, dtype=jnp.int32)[None, :]).astype(
        jnp.int32
    )
    earlier = jnp.cumsum(onehot, axis=0) - onehot
    places = jnp.sum(earlier * onehot, axis=1)
    slot_ids = (flat_ids * capacity + places).reshape(row_count, top_count)
    slot_range = jnp.arange(expert_count * capacity, dtype=jnp.int32)
    dispatch = jnp.any(slot_range[:, None, None] == slot_ids[None, :, :], axis=-1).astype(
        jnp.bfloat16
    )
    outgoing = jnp.dot(dispatch, normed, preferred_element_type=jnp.float32).astype(jnp.bfloat16)
    outgoing = outgoing.reshape(expert_count, capacity, model_width)
    arrived = lax.all_to_all(outgoing, ("fs", "tp"), split_axis=0, concat_axis=0, tiled=True)
    source_count, slot_count, width_here = arrived.shape
    arrived_rows = arrived.reshape(source_count * slot_count, width_here)
    hidden = gated(arrived_rows, gate_up).astype(jnp.bfloat16)
    result = jnp.dot(hidden, lowered, preferred_element_type=jnp.float32).astype(jnp.bfloat16)
    result = result.reshape(source_count, slot_count, width_here)
    returned = lax.all_to_all(result, ("fs", "tp"), split_axis=0, concat_axis=0, tiled=True)
    picked = returned.reshape(expert_count * capacity, model_width)[slot_ids]
    routed = jnp.sum(route_weight[:, :, None] * picked.astype(jnp.float32), axis=1)
    return (routed + shared_sum).astype(jnp.bfloat16)


def body(
    prompt,
    train_gate,
    train_up,
    train_down,
    train_shared_gate,
    train_shared_up,
    train_shared_down,
    norm_gain,
    expert_ids,
    route_weight,
):
    widened = prompt.astype(jnp.float32)
    normed = (
        widened * lax.rsqrt(jnp.mean(widened * widened, axis=-1, keepdims=True) + eps_norm)
    ).astype(jnp.bfloat16)
    gained_gate = jnp.swapaxes(train_gate, 1, 2) * norm_gain
    gained_up = jnp.swapaxes(train_up, 1, 2) * norm_gain
    stacked = to_owners(jnp.stack((gained_gate, gained_up), axis=1).astype(jnp.bfloat16))
    lowered = to_owners(train_down.astype(jnp.bfloat16)[:, None])
    shared = jnp.stack(
        (
            train_shared_gate.T * norm_gain,
            train_shared_up.T * norm_gain,
            train_shared_down,
            jnp.zeros_like(train_shared_down),
        )
    ).astype(jnp.bfloat16)
    shared = lax.all_gather(shared, ("gr", "fs"), axis=0)
    shared = shared[:, :3].transpose(1, 2, 0, 3).reshape(3, train_shared_down.shape[0], -1)
    model_width = prompt.shape[1]
    mix = (
        dense_mix
        if lax.axis_size("fs") * lax.axis_size("tp") <= 2 * expert_ids.shape[1]
        else sparse_mix
    )
    mixed_out = mix(
        normed,
        expert_ids,
        route_weight,
        stacked.reshape(-1, model_width),
        lowered[0],
        shared[:2].reshape(-1, model_width),
        shared[2],
    )
    return (
        jnp.swapaxes(stacked[:1], 1, 2),
        jnp.swapaxes(stacked[1:], 1, 2),
        lowered,
        shared[0].T,
        shared[1].T,
        shared[2],
        mixed_out,
    )


def solution(mesh):
    placed = (
        P(("gr", "fs", "tp"), None),
        P(None, ("gr", "fs"), "tp"),
        P(None, ("gr", "fs"), "tp"),
        P(None, "tp", ("gr", "fs")),
        P(("gr", "fs"), "tp"),
        P(("gr", "fs"), "tp"),
        P("tp", ("gr", "fs")),
        P(("gr", "fs")),
        P(("gr", "fs", "tp"), None),
        P(("gr", "fs", "tp"), None),
    )
    return jax.shard_map(
        body,
        mesh=mesh,
        in_specs=placed,
        out_specs=(
            P(("fs", "tp"), None, None),
            P(("fs", "tp"), None, None),
            P(("fs", "tp"), None, None),
            P(None, "tp"),
            P(None, "tp"),
            P("tp", None),
            P(("gr", "fs", "tp"), None),
        ),
        check_vma=False,
    )
```

profile of v0, /device:TPU:0, one launch (start us, length us, event | category | flops | bytes accessed | tf_op | source)
XLA Modules:
  0.0 323.8 jit_solution(4078553129348858008)
XLA Ops:
  7.2 1.0 convert_bitcast_fusion.1
  8.3 0.9 fusion.9
  10.8 1.2 fusion.4
  12.1 1.2 fusion.5
  13.3 0.9 pad_maximum_fusion.2
  14.6 43.9 %all_to_all.10 = bf16[16,2,64,256]{3,2,1,0:T(8,128)(2,1)S(1)} all-to-all(bf16[16,2,64,256]{3,2,1,0:T(8,128)(2,1)S(1)} %pad_maximum_fusion.1), channel_id=1, replica_groups=mesh['gr'=2,'fs'=4,'tp'=4] {'fs','tp'}, dimensions={0} | all-to-all | bytes 2097152 | tf_op jit(solution)/shard_map/all_to_all | solution.py:13
  59.3 1.5 reshape.162
  60.9 0.9 convert_bitcast_fusion
  61.7 5.1 %all-to-all-start.1 = ((bf16[16,1,64,256]{3,2,1,0:T(8,128)(2,1)}), bf16[16,1,64,256]{3,2,1,0:T(8,128)(2,1)S(1)}, u32[]{:S(2)}, u32[]{:S(2)}) async-start(bf16[16,1,64,256]{3,2,1,0:T(8,128)(2,1)} %convert_bitcast_fusion), calls=%async_computation.1 | async-start | bytes 1048576 | tf_op jit(solution)/shard_map/all_to_all | solution.py:13
  66.9 21.5 %all-to-all-done.1 = bf16[16,1,64,256]{3,2,1,0:T(8,128)(2,1)S(1)} async-done(((bf16[16,1,64,256]{3,2,1,0:T(8,128)(2,1)}), bf16[16,1,64,256]{3,2,1,0:T(8,128)(2,1)S(1)}, u32[]{:S(2)}, u32[]{:S(2)}) %all-to-all-start.1) | async-done | bytes 524320 | tf_op jit(solution)/shard_map/all_to_all | solution.py:13
  88.8 1.2 reshape.164
  90.1 1.2 slice_bitcast_fusion.2
  91.8 55.9 %all-gather.12.cloned.1.call-done = bf16[2176,2048]{1,0:T(8,128)(2,1)} async-done(((bf16[136,2048]{1,0:T(8,128)(2,1)}), bf16[2176,2048]{1,0:T(8,128)(2,1)}) %all-gather.12.cloned.1.call-update) | async-done | bytes 8912912 | tf_op jit(solution)/shard_map/all_gather | solution.py:41
  147.7 1.1 slice.82
  148.8 1.8 constant_dynamic-slice_fusion
  152.1 29.4 %all-gather.6.cloned.1.call-done = bf16[2,256,2048]{2,1,0:T(8,128)(2,1)} async-done(((bf16[2,256,1024]{2,1,0:T(8,128)(2,1)}), bf16[2,256,2048]{2,1,0:T(8,128)(2,1)}) %all-gather.6.cloned.1.call-update) | async-done | bytes 2097168 | tf_op jit(solution)/shard_map/all_gather | solution.py:16
  181.5 8.0 %fusion.14 = f32[2176,512]{1,0:T(8,128)S(1)} fusion(bf16[2176,2048]{1,0:T(8,128)(2,1)} %all-gather.12.cloned.1.call-done, bf16[512,2048]{1,0:T(8,128)(2,1)} %bitcast.84), kind=kOutput, calls=%fused_computation.45 | convolution fusion | flops 4563402752 | bytes 15466496 | tf_op jit(solution)/shard_map/dot_general | solution.py:20
  190.7 14.1 %all-gather.8.cloned.1.call-done = bf16[1,256,2048]{2,1,0:T(8,128)(2,1)} async-done(((bf16[1,256,1024]{2,1,0:T(8,128)(2,1)}), bf16[1,256,2048]{2,1,0:T(8,128)(2,1)}) %all-gather.8.cloned.1.call-update) | async-done | bytes 1048592 | tf_op jit(solution)/shard_map/all_gather | solution.py:16
  204.8 7.9 %convolution_convert_fusion = bf16[2048,2048]{1,0:T(8,128)(2,1)} fusion(bf16[2048,320]{1,0:T(8,128)(2,1)S(1)} %bitcast.88, bf16[64,2048]{1,0:T(8,128)(2,1)S(1)} %bitcast.97, bf16[256,2048]{1,0:T(8,128)(2,1)} %bitcast.89), kind=kOutput, calls=%fused_computation | convolution fusion | flops 2691170304 | bytes 11010048 | tf_op jit(solution)/shard_map/dot_general | solution.py:57
  214.1 1.7 slice_bitcast_fusion
  215.8 1.3 copy.60
  217.1 1.3 copy.61
  218.4 97.8 %reduce-scatter.2.cloned.1.call-done = bf16[128,2048]{1,0:T(8,128)(2,1)} async-done(((bf16[2048,2048]{1,0:T(8,128)(2,1)}), bf16[128,2048]{1,0:T(8,128)(2,1)}) %reduce-scatter.2.cloned.1.call-update) | async-done | bytes 524304 | tf_op jit(solution)/shard_map/reduce_scatter | solution.py:58
  316.3 1.0 copy.75
  (54 shorter events, 8.0 us)
Async XLA Ops:
  7.2 7.0 %copy-start.5 = (f32[256]{0:T(256)S(1)}, f32[256]{0:T(256)}, u32[]{:S(2)}) copy-start(f32[256]{0:T(256)} %param.17) | copy-start | bytes 3076
  7.2 7.0 %copy-start.1 = (f32[16,256,64]{1,2,0:T(8,128)S(1)}, f32[16,256,64]{1,2,0:T(8,128)}, u32[]{:S(2)}) copy-start(f32[16,256,64]{1,2,0:T(8,128)} %param.11) | copy-start | bytes 3145732
  7.2 7.0 %copy-start.2 = (f32[16,256,64]{1,2,0:T(8,128)S(1)}, f32[16,256,64]{1,2,0:T(8,128)}, u32[]{:S(2)}) copy-start(f32[16,256,64]{1,2,0:T(8,128)} %param.12) | copy-start | bytes 3145732
  7.2 82.9 %all-gather.10.cloned.1.call-start = ((), (), s32[]{:S(2)}) async-start(), calls=%async_computation.5 | async-start | bytes 1179648 | tf_op jit(solution)/shard_map/all_gather | solution.py:127
  10.0 137.8 %all-gather.12.cloned.1.call-start = ((), (), s32[]{:S(2)}) async-start(), calls=%async_computation.7 | async-start | bytes 9469952 | tf_op jit(solution)/shard_map/all_gather | solution.py:41
  14.1 167.3 %all-gather.6.cloned.1.call-start = ((), (), s32[]{:S(2)}) async-start(), calls=%async_computation.3 | async-start | bytes 3145728 | tf_op jit(solution)/shard_map/all_gather | solution.py:16
  58.5 2.4 copy-start
  61.7 26.7 %all-to-all-start.1 = ((bf16[16,1,64,256]{3,2,1,0:T(8,128)(2,1)}), bf16[16,1,64,256]{3,2,1,0:T(8,128)(2,1)S(1)}, u32[]{:S(2)}, u32[]{:S(2)}) async-start(bf16[16,1,64,256]{3,2,1,0:T(8,128)(2,1)} %convert_bitcast_fusion), calls=%async_computation.1 | async-start | bytes 1048576 | tf_op jit(solution)/shard_map/all_to_all | solution.py:13
  66.8 137.9 %all-gather.8.cloned.1.call-start = ((), (), s32[]{:S(2)}) async-start(), calls=%async_computation.4 | async-start | bytes 1572864 | tf_op jit(solution)/shard_map/all_gather | solution.py:16
  90.0 226.3 %reduce-scatter.2.cloned.1.call-start = ((), (), s32[]{:S(2)}) async-start(), calls=%async_computation.6 | async-start | bytes 8912896 | tf_op jit(solution)/shard_map/reduce_scatter | solution.py:58
  91.8 112.9 %copy-start.4 = (bf16[8,8,8,256]{3,1,2,0:T(8,128)(2,1)}, bf16[8,8,8,256]{3,1,2,0:T(8,128)(2,1)S(1)}, u32[]{:S(2)}) copy-start(bf16[8,8,8,256]{3,1,2,0:T(8,128)(2,1)S(1)} %copy.64) | copy-start | bytes 786436
  215.8 100.5 %copy-start.3 = (bf16[1,256,2048]{2,1,0:T(8,128)(2,1)S(1)}, bf16[1,256,2048]{2,1,0:T(8,128)(2,1)}, u32[]{:S(2)}) copy-start(bf16[1,256,2048]{2,1,0:T(8,128)(2,1)} %all-gather.8.cloned.1.call-done) | copy-start | bytes 3145732
Sparse Core Ops, SparseCore 0:
  10.7 48.1 all-gather.9
  61.8 85.8 all-gather.11
  149.8 31.5 all-gather.5
  183.4 21.2 all-gather.7
  212.8 103.4 reduce-scatter.1
where the time goes:
time: 324 us
  waiting for transfers between devices  219 us (68%)
  blocking collectives  43.9 us (14%)
  matrix products  16.7 us (5%)
  local copies, waits for them, and re-layouts  15.8 us (5%)
  between operations  14.1 us (4%)
  other arithmetic  9.15 us (3%)
  starting transfers between devices  5.29 us (2%)
    reduce_scatter x1, waiting for transfers between devices, dense_mix(): lax.psum_scatter(partial, ('fs', 'tp'), scatter_dimension=0, tiled=True)  97.8 us
    all_gather x1, waiting for transfers between devices, dense_mix(): lax.all_gather(jnp.concatenate((normed, coded), axis=0), ('fs', 'tp'), ax...  55.9 us
    all_to_all x1, blocking collectives, to_owners(): lax.all_to_all(pieces, ('fs', 'tp'), split_axis=0, concat_axis=0, tiled=T...  43.9 us
    all_gather x2, waiting for transfers between devices, to_owners(): return lax.all_gather(pieces, 'gr', axis=2, tiled=True)  43.5 us
    all_to_all x1, waiting for transfers between devices, to_owners(): lax.all_to_all(pieces, ('fs', 'tp'), split_axis=0, concat_axis=0, tiled=T...  21.5 us
    dot_general x2, matrix products, dot_last(): lax.dot_general(left, right, (((1,), (1,)), ((), ())), preferred_element_...  8.8 us
    dot_general x1, matrix products, dense_mix(): jnp.dot(act, down, preferred_element_type=jnp.float32).astype(jnp.bfloat16)  7.9 us
  transfers between devices with their start and end apart: 6, of which 5 were waited for; matrix products, arithmetic and copies ran while one was open for 9% of the time, Pallas kernels for 0%

commit v1 on v0

--- a/solution.py
+++ b/solution.py
@@ -1,3 +1,4 @@
+import functools
 import jax
 import jax.numpy as jnp
 from jax import lax
@@ -7,13 +8,20 @@
 row_tile = 8
 
 
+def choose_shards(block_here, along_axis, where_dim):
+    return jnp.concatenate(lax.all_gather(block_here, axis_name=along_axis), where_dim)
+
+
+strips_all_apply = functools.partial(choose_shards, along_axis="gr", where_dim=2)
+
+
 def to_owners(pieces):
     count, kinds, hidden_part, width_part = pieces.shape
     fs, tp = (lax.axis_size("fs"), lax.axis_size("tp"))
     pieces = lax.all_to_all(pieces, ("fs", "tp"), split_axis=0, concat_axis=0, tiled=True)
     pieces = pieces.reshape(fs, tp, kinds, hidden_part, width_part)
     pieces = pieces.transpose(2, 1, 3, 0, 4).reshape(kinds, tp * hidden_part, fs * width_part)
-    return lax.all_gather(pieces, "gr", axis=2, tiled=True)
+    return strips_all_apply(pieces)
 
 
 def dot_last(left, right):

time: 324 us -> 337 us (1.040)
  blocking collectives: 43.9 us -> 0 us
  waiting for transfers between devices: 219 us -> 259 us
  local copies, waits for them, and re-layouts: 15.8 us -> 30.9 us
  starting transfers between devices: 5.29 us -> 12 us
  matrix products: 16.7 us -> 12.7 us
    all_to_all x1 -> x0, blocking collectives: 43.9 us -> none  [to_owners(): lax.all_to_all(pieces, ('fs', 'tp'), split_axis=0, concat_axis=0, tiled=T...]
    all_gather x1, waiting for transfers between devices: 55.9 us -> 74.6 us  [dense_mix(): lax.all_gather(jnp.concatenate((normed, coded), axis=0), ('fs', 'tp'), ax...]
    all_to_all x1 -> x2, waiting for transfers between devices: 21.5 us -> 38.2 us  [to_owners(): lax.all_to_all(pieces, ('fs', 'tp'), split_axis=0, concat_axis=0, tiled=T...]
    all_gather x2, waiting for transfers between devices: 43.5 us -> 53.2 us  [choose_shards(): lax.all_gather(block_here, axis_name=along_axis)]
    reduce_scatter x1, waiting for transfers between devices: 97.8 us -> 90.4 us  [dense_mix(): lax.psum_scatter(partial, ('fs', 'tp'), scatter_dimension=0, tiled=True)]
    all_to_all x1 -> x2, starting transfers between devices: 5.08 us -> 11.6 us  [to_owners(): lax.all_to_all(pieces, ('fs', 'tp'), split_axis=0, concat_axis=0, tiled=T...]
    unnamed x22 -> x35, local copies, waits for them, and re-layouts: 5.5 us -> 10.2 us
    all_gather x0 -> x2, local copies, waits for them, and re-layouts: none -> 4.1 us  [choose_shards(): lax.all_gather(block_here, axis_name=along_axis)]
  transfers between devices with their start and end apart: 6 -> 7, of which waited for: 5 -> 7; matrix products, arithmetic and copies ran while one was open for 9% -> 9% of each run, Pallas kernels for 0% -> 0%
where the time goes in v1:
time: 337 us; the launch traced here: 336 us
  waiting for transfers between devices  259 us (77%)
  local copies, waits for them, and re-layouts  30.9 us (9%)
  between operations  14.2 us (4%)
  matrix products  12.7 us (4%)
  starting transfers between devices  12 us (4%)
  other arithmetic  6.82 us (2%)
    reduce_scatter x1, waiting for transfers between devices, dense_mix(): lax.psum_scatter(partial, ('fs', 'tp'), scatter_dimension=0, tiled=True)  90.4 us
    all_gather x1, waiting for transfers between devices, dense_mix(): lax.all_gather(jnp.concatenate((normed, coded), axis=0), ('fs', 'tp'), ax...  74.6 us
    all_gather x2, waiting for transfers between devices, choose_shards(): lax.all_gather(block_here, axis_name=along_axis)  53.2 us
    all_to_all x2, waiting for transfers between devices, to_owners(): lax.all_to_all(pieces, ('fs', 'tp'), split_axis=0, concat_axis=0, tiled=T...  38.2 us
    all_to_all x2, starting transfers between devices, to_owners(): lax.all_to_all(pieces, ('fs', 'tp'), split_axis=0, concat_axis=0, tiled=T...  11.6 us
    unnamed x35, local copies, waits for them, and re-layouts  10.2 us
    dot_general x1, matrix products, dense_mix(): jnp.dot(act, down, preferred_element_type=jnp.float32).astype(jnp.bfloat16)  7.1 us
  transfers between devices with their start and end apart: 7, of which 7 were waited for; matrix products, arithmetic and copies ran while one was open for 9% of the time, Pallas kernels for 0%

profile of v1, /device:TPU:0, one launch (start us, length us, event | category | flops | bytes accessed | tf_op | source)
XLA Modules:
  0.0 336.1 jit_solution(124361531711967149)
XLA Ops:
  7.2 2.2 convert_bitcast_fusion
  9.5 7.4 %all-to-all-start.1 = ((bf16[16,1,64,256]{3,2,1,0:T(8,128)(2,1)}), bf16[16,1,64,256]{3,2,1,0:T(8,128)(2,1)S(1)}, u32[]{:S(2)}, u32[]{:S(2)}) async-start(bf16[16,1,64,256]{3,2,1,0:T(8,128)(2,1)} %convert_bitcast_fusion), calls=%async_computation.1 | async-start | bytes 1048576 | tf_op jit(solution)/shard_map/all_to_all | solution.py:21
  19.1 12.0 %all-to-all-done.1 = bf16[16,1,64,256]{3,2,1,0:T(8,128)(2,1)S(1)} async-done(((bf16[16,1,64,256]{3,2,1,0:T(8,128)(2,1)}), bf16[16,1,64,256]{3,2,1,0:T(8,128)(2,1)S(1)}, u32[]{:S(2)}, u32[]{:S(2)}) %all-to-all-start.1) | async-done | bytes 524320 | tf_op jit(solution)/shard_map/all_to_all | solution.py:21
  31.2 4.2 %all-to-all-start = ((bf16[16,2,64,256]{3,2,1,0:T(8,128)(2,1)}), bf16[16,2,64,256]{3,2,1,0:T(8,128)(2,1)S(1)}, u32[]{:S(2)}, u32[]{:S(2)}) async-start(bf16[16,2,64,256]{3,2,1,0:T(8,128)(2,1)} %pad_maximum_fusion.1), calls=%async_computation | async-start | bytes 2097152 | tf_op jit(solution)/shard_map/all_to_all | solution.py:21
  35.8 1.2 all_gather_reshape.7
  37.0 26.2 %all-to-all-done = bf16[16,2,64,256]{3,2,1,0:T(8,128)(2,1)S(1)} async-done(((bf16[16,2,64,256]{3,2,1,0:T(8,128)(2,1)}), bf16[16,2,64,256]{3,2,1,0:T(8,128)(2,1)S(1)}, u32[]{:S(2)}, u32[]{:S(2)}) %all-to-all-start) | async-done | bytes 1048608 | tf_op jit(solution)/shard_map/all_to_all | solution.py:21
  64.0 1.5 all_gather_reshape.6
  67.3 3.0 all-gather.10.cloned.1.call-done
  70.3 1.2 slice_bitcast_fusion
  73.0 19.4 %all-gather.8.cloned.1.call-done = bf16[2,1,256,1024]{3,2,1,0:T(8,128)(2,1)} async-done(((bf16[1,1,256,1024]{3,2,1,0:T(8,128)(2,1)}), bf16[2,1,256,1024]{3,2,1,0:T(8,128)(2,1)}) %all-gather.8.cloned.1.call-update) | async-done | bytes 1048592 | tf_op jit(solution)/shard_map/all_gather | solution.py:12
  92.4 1.5 copy.78
  93.9 33.8 %all-gather.6.cloned.1.call-done = bf16[2,2,256,1024]{3,2,1,0:T(8,128)(2,1)} async-done(((bf16[1,2,256,1024]{3,2,1,0:T(8,128)(2,1)}), bf16[2,2,256,1024]{3,2,1,0:T(8,128)(2,1)}) %all-gather.6.cloned.1.call-update) | async-done | bytes 2097168 | tf_op jit(solution)/shard_map/all_gather | solution.py:12
  127.7 3.7 %copy.82 = bf16[2,256,2,1024]{3,2,1,0:T(2,128)(2,1)S(1)} copy(bf16[2,256,2,1024]{3,1,0,2:T(8,128)(2,1)} %bitcast.89) | data formatting | bytes 4194304 | tf_op jit(solution)/shard_map/reshape | solution.py:12
  131.4 2.0 copy.89
  133.5 74.6 %all-gather.12.cloned.1.call-done = bf16[2176,2048]{1,0:T(8,128)(2,1)} async-done(((bf16[136,2048]{1,0:T(8,128)(2,1)}), bf16[2176,2048]{1,0:T(8,128)(2,1)}) %all-gather.12.cloned.1.call-update) | async-done | bytes 8912912 | tf_op jit(solution)/shard_map/all_gather | solution.py:49
  209.1 1.9 constant_dynamic-slice_fusion
  214.2 4.8 %fusion.15 = f32[2176,512]{1,0:T(8,128)S(1)} fusion(bf16[2176,2048]{1,0:T(8,128)(2,1)S(1)} %copy-done.6, bf16[512,2048]{1,0:T(8,128)(2,1)S(1)} %bitcast.99), kind=kOutput, calls=%fused_computation.45 | convolution fusion | flops 4563402752 | bytes 15466496 | tf_op jit(solution)/shard_map/dot_general | solution.py:28
  220.3 7.1 %convolution_convert_fusion = bf16[2048,2048]{1,0:T(8,128)(2,1)} fusion(bf16[2048,320]{1,0:T(8,128)(2,1)S(1)} %bitcast.104, bf16[64,2048]{0,1:T(8,128)(2,1)S(1)} %bitcast.97, bf16[256,2048]{0,1:T(8,128)(2,1)S(1)} %bitcast.92), kind=kOutput, calls=%fused_computation | convolution fusion | flops 2691170304 | bytes 11010048 | tf_op jit(solution)/shard_map/dot_general | solution.py:65
  227.4 2.1 copy.85
  229.5 1.7 copy.87
  231.9 1.4 copy.84
  233.3 2.6 copy.76
  235.9 3.2 fusion.13
  239.1 90.4 %reduce-scatter.2.cloned.1.call-done = bf16[128,2048]{1,0:T(8,128)(2,1)} async-done(((bf16[2048,2048]{1,0:T(8,128)(2,1)}), bf16[128,2048]{1,0:T(8,128)(2,1)}) %reduce-scatter.2.cloned.1.call-update) | async-done | bytes 524304 | tf_op jit(solution)/shard_map/reduce_scatter | solution.py:66
  (72 shorter events, 12.7 us)
Async XLA Ops:
  7.2 9.8 %copy-start.9 = (f32[64,256]{1,0:T(8,128)S(1)}, f32[64,256]{1,0:T(8,128)}, u32[]{:S(2)}) copy-start(f32[64,256]{1,0:T(8,128)} %param.16) | copy-start | bytes 196612
  7.2 9.9 %copy-start.7 = (f32[256,64]{0,1:T(8,128)S(1)}, f32[256,64]{0,1:T(8,128)}, u32[]{:S(2)}) copy-start(f32[256,64]{0,1:T(8,128)} %param.14) | copy-start | bytes 196612
  7.2 9.9 %copy-start.8 = (f32[256,64]{0,1:T(8,128)S(1)}, f32[256,64]{0,1:T(8,128)}, u32[]{:S(2)}) copy-start(f32[256,64]{0,1:T(8,128)} %param.15) | copy-start | bytes 196612
  7.2 9.8 %copy-start.10 = (f32[256]{0:T(256)S(1)}, f32[256]{0:T(256)}, u32[]{:S(2)}) copy-start(f32[256]{0:T(256)} %param.17) | copy-start | bytes 3076
  7.2 10.6 %copy-start.4 = (f32[16,256,64]{1,2,0:T(8,128)S(1)}, f32[16,256,64]{1,2,0:T(8,128)}, u32[]{:S(2)}) copy-start(f32[16,256,64]{1,2,0:T(8,128)} %param.11) | copy-start | bytes 3145732
  7.2 10.6 %copy-start.5 = (f32[16,256,64]{1,2,0:T(8,128)S(1)}, f32[16,256,64]{1,2,0:T(8,128)}, u32[]{:S(2)}) copy-start(f32[16,256,64]{1,2,0:T(8,128)} %param.12) | copy-start | bytes 3145732
  9.5 21.7 %all-to-all-start.1 = ((bf16[16,1,64,256]{3,2,1,0:T(8,128)(2,1)}), bf16[16,1,64,256]{3,2,1,0:T(8,128)(2,1)S(1)}, u32[]{:S(2)}, u32[]{:S(2)}) async-start(bf16[16,1,64,256]{3,2,1,0:T(8,128)(2,1)} %convert_bitcast_fusion), calls=%async_computation.1 | async-start | bytes 1048576 | tf_op jit(solution)/shard_map/all_to_all | solution.py:21
  16.9 53.4 %all-gather.10.cloned.1.call-start = ((), (), s32[]{:S(2)}) async-start(), calls=%async_computation.5 | async-start | bytes 1179648 | tf_op jit(solution)/shard_map/all_gather | solution.py:135
  31.2 32.1 %all-to-all-start = ((bf16[16,2,64,256]{3,2,1,0:T(8,128)(2,1)}), bf16[16,2,64,256]{3,2,1,0:T(8,128)(2,1)S(1)}, u32[]{:S(2)}, u32[]{:S(2)}) async-start(bf16[16,2,64,256]{3,2,1,0:T(8,128)(2,1)} %pad_maximum_fusion.1), calls=%async_computation | async-start | bytes 2097152 | tf_op jit(solution)/shard_map/all_to_all | solution.py:21
  35.3 57.1 %all-gather.8.cloned.1.call-start = ((), (), s32[]{:S(2)}) async-start(), calls=%async_computation.4 | async-start | bytes 1572864 | tf_op jit(solution)/shard_map/all_gather | solution.py:12
  37.0 90.7 %all-gather.6.cloned.1.call-start = ((), (), s32[]{:S(2)}) async-start(), calls=%async_computation.3 | async-start | bytes 3145728 | tf_op jit(solution)/shard_map/all_gather | solution.py:12
  63.2 2.4 copy-start.11
  63.2 2.5 copy-start.12
  63.2 2.6 copy-start.3
  65.6 142.4 %all-gather.12.cloned.1.call-start = ((), (), s32[]{:S(2)}) async-start(), calls=%async_computation.7 | async-start | bytes 9469952 | tf_op jit(solution)/shard_map/all_gather | solution.py:49
  67.0 262.5 %reduce-scatter.2.cloned.1.call-start = ((), (), s32[]{:S(2)}) async-start(), calls=%async_computation.6 | async-start | bytes 8912896 | tf_op jit(solution)/shard_map/reduce_scatter | solution.py:66
  73.0 147.3 %copy-start.1 = (bf16[1,64,8,256]{1,3,2,0:T(8,128)(2,1)}, bf16[1,64,8,256]{1,3,2,0:T(8,128)(2,1)S(1)}, u32[]{:S(2)}) copy-start(bf16[1,64,8,256]{1,3,2,0:T(8,128)(2,1)S(1)} %copy.81) | copy-start | bytes 786436
  209.1 4.2 %copy-start.6 = (bf16[2176,2048]{1,0:T(8,128)(2,1)S(1)}, bf16[2176,2048]{1,0:T(8,128)(2,1)}, u32[]{:S(2)}) copy-start(bf16[2176,2048]{1,0:T(8,128)(2,1)} %all-gather.12.cloned.1.call-done) | copy-start | bytes 26738692
  211.8 2.3 copy-start.2
  227.4 5.9 %copy-start = (bf16[2,2,256,1024]{3,2,1,0:T(8,128)(2,1)S(1)}, bf16[2,2,256,1024]{3,2,1,0:T(8,128)(2,1)}, u32[]{:S(2)}) copy-start(bf16[2,2,256,1024]{3,2,1,0:T(8,128)(2,1)} %all-gather.6.cloned.1.call-done) | copy-start | bytes 6291460
Sparse Core Ops, SparseCore 0:
  20.4 49.8 all-gather.9
  72.4 19.9 all-gather.7
  94.6 33.0 all-gather.5
  130.4 77.5 all-gather.11
  227.5 101.9 reduce-scatter.1
